TPU v7x, 32 devices: a whole 2x2x4 slice. The times are simulated.
32 devices in a mesh: kv: 8 (over z, y), tp: 4 (over x, core).
Axes of the slice: x: 2, y: 2, z: 4, core: 2. Of those that a mesh axis runs over, the one named last changes fastest.
Arguments:
- tokens: bfloat16 [16, 16, 4096], replicated, may hold values from -6 to 6
- gain_pre: float32 [4096], replicated, may hold values from 0.1 to 1.9
- w_query: bfloat16 [4096, 2048], P('kv', 'tp'), may hold values from -0.09375 to 0.09375
- w_key: bfloat16 [4096, 2048], P('kv', 'tp'), may hold values from -0.09375 to 0.09375
- w_value: bfloat16 [4096, 2048], P('kv', 'tp'), may hold values from -0.09375 to 0.09375
- w_forget: bfloat16 [4096, 16], replicated, may hold values from -0.09375 to 0.09375
- b_forget: float32 [16], replicated
- w_out: bfloat16 [2048, 4096], P('tp', 'kv'), may hold values from -0.125 to 0.125
- gain_post: float32 [4096], P(('kv', 'tp')), may hold values from 0.1 to 1.9
- key_cache: bfloat16 [16, 1024, 16, 128], P(None, 'kv', 'tp'), may hold values from -6 to 6
- value_cache: bfloat16 [16, 1024, 16, 128], P(None, 'kv', 'tp'), may hold values from -6 to 6
- cum_cache: float32 [16, 1024, 16], P(None, 'kv', 'tp'), may hold values from -402 to 0, as said below
- lengths: int32 [16], replicated, may hold values from 512 to 992
- accepted: int32 [16], replicated, may hold values from 0 to 16
- parent: int32 [16, 16], replicated, may hold values from -1 to 14, as said below
Outputs:
- mixed: bfloat16 [16, 16, 4096], P(None, None, ('kv', 'tp'))
- key_out: bfloat16 [16, 1024, 16, 128], P(None, 'kv', 'tp')
- value_out: bfloat16 [16, 1024, 16, 128], P(None, 'kv', 'tp')
- cum_out: float32 [16, 1024, 16], P(None, 'kv', 'tp')
Inputs may be any that keep to these rules, and one draw needn't show every extreme that they name: parent[s, 0] is -1 and parent[s, i] lies between -1 and i - 1. `cum_cache`: along the positions of each sequence and head the values never rise. lengths + accepted + 16 never exceeds 1024.
All inputs are finite; a program needn't handle non-finite values.
Results may differ from a plain program's by a relative error of at most 0.03.
Values may be sent and summed in bfloat16 or wider, within the bound.
No kernel may reach another device: no remote copies, remote signals or barrier semaphores. Data moves between devices by JAX's collectives and lax.ppermute only.
A program may use at most 64 MiB of HBM per device.

v0:
```python
import jax
import jax.numpy as jnp
from jax import lax
from jax.sharding import PartitionSpec as P

epsilon = 1e-06
floor_value = -1e30


def merged(part, axis, combine):
    gathered = jax.tree.map(lambda a: lax.all_gather(a, axis), part)

    def take(source):
        return jax.tree.map(lambda a: lax.dynamic_index_in_dim(a, source, 0, False), gathered)

    return lax.fori_loop(
        1, lax.axis_size(axis), lambda source, state: combine(state, take(source)), take(0)
    )


def ancestry(parent_ids, members):
    identity = jnp.eye(members, dtype=jnp.float32)
    parent_hot = (
        parent_ids[:, :, None] == jnp.arange(members, dtype=jnp.int32)[None, None, :]
    ).astype(jnp.float32)
    ancestors = jnp.minimum(identity[None] + parent_hot, 1.0)
    for sweep in range(max(1, (members - 1).bit_length())):
        ancestors = jnp.minimum(
            jnp.einsum("bij,bjk->bik", ancestors, ancestors, precision=lax.Precision.HIGHEST), 1.0
        )
    return ancestors


def combine_parts(first, second):
    new_max = jnp.maximum(first[0], second[0])
    first_scale = jnp.exp(first[0] - new_max)
    second_scale = jnp.exp(second[0] - new_max)
    return (
        new_max,
        first[1] * first_scale + second[1] * second_scale,
        first[2] * first_scale[..., None] + second[2] * second_scale[..., None],
        jnp.maximum(first[3], second[3]),
    )


def finish_rows(cache_max, cache_total, cache_values, last_rows, tree_max, tree_total, tree_values):
    shifted = cache_max + last_rows
    top = jnp.maximum(shifted, tree_max)
    cache_scale = jnp.exp(shifted - top)
    tree_scale = jnp.exp(tree_max - top)
    attended = (
        (cache_values * cache_scale[..., None] + tree_values * tree_scale[..., None])
        / (cache_total * cache_scale + tree_total * tree_scale)[..., None]
    ).astype(jnp.bfloat16)
    return attended.reshape(attended.shape[0], attended.shape[1] * attended.shape[2])


def per_device(
    tokens,
    gain_pre,
    w_query,
    w_key,
    w_value,
    w_forget,
    b_forget,
    w_out,
    gain_post,
    key_cache,
    value_cache,
    cum_cache,
    lengths,
    accepted,
    parent,
):
    num_seqs, proposals, model_width = tokens.shape
    kv_rank = lax.axis_index("kv")
    tp_rank = lax.axis_index("tp")
    span = key_cache.shape[1]
    heads_local = key_cache.shape[2]
    head_dim = key_cache.shape[3]
    scale = head_dim ** (-0.5)
    all_rows = num_seqs * proposals
    tok_float = tokens.astype(jnp.float32)
    normed = (
        tok_float
        * lax.rsqrt(jnp.mean(tok_float * tok_float, -1, keepdims=True) + epsilon)
        * gain_pre
    ).astype(jnp.bfloat16)
    flat = normed.reshape(all_rows, model_width)
    weight_rows = w_query.shape[0]
    local_rows = lax.dynamic_slice_in_dim(flat, kv_rank * weight_rows, weight_rows, 1)
    query_part = jnp.dot(local_rows, w_query, preferred_element_type=jnp.float32)
    key_part = jnp.dot(local_rows, w_key, preferred_element_type=jnp.float32)
    value_part = jnp.dot(local_rows, w_value, preferred_element_type=jnp.float32)
    summed = (
        lax.psum(query_part.astype(jnp.bfloat16), "kv").astype(jnp.float32),
        lax.psum(key_part.astype(jnp.bfloat16), "kv").astype(jnp.float32),
        lax.psum(value_part.astype(jnp.bfloat16), "kv").astype(jnp.float32),
    )
    query_flat = summed[0].astype(jnp.bfloat16)
    key_flat = summed[1].astype(jnp.bfloat16)
    value_flat = summed[2].astype(jnp.bfloat16)
    query = query_flat.reshape(num_seqs, proposals, heads_local, head_dim)
    key_new = key_flat.reshape(num_seqs, proposals, heads_local, head_dim)
    value_new = value_flat.reshape(num_seqs, proposals, heads_local, head_dim)
    forget_cols = lax.dynamic_slice_in_dim(w_forget, tp_rank * heads_local, heads_local, 1)
    forget_bias = lax.dynamic_slice_in_dim(b_forget, tp_rank * heads_local, heads_local, 0)
    log_forget = jax.nn.log_sigmoid(
        jnp.dot(flat, forget_cols, preferred_element_type=jnp.float32) + forget_bias
    ).reshape(num_seqs, proposals, heads_local)
    ancestors = ancestry(parent, proposals)
    path = jnp.einsum("bij,bjh->bih", ancestors, log_forget, precision=lax.Precision.HIGHEST)
    valid = lengths + accepted
    positions = kv_rank * span + jnp.arange(span, dtype=jnp.int32)
    live = (positions[None, :] < valid[:, None])[:, None, None, :]
    score = (
        jnp.einsum("bihd,bkhd->bihk", query, key_cache, preferred_element_type=jnp.float32) * scale
        + path[..., None]
        - jnp.swapaxes(cum_cache, 1, 2)[:, None]
    )
    block_max = jnp.max(jnp.where(live, score, floor_value), axis=-1)
    weight = jnp.exp(jnp.where(live, score - block_max[..., None], floor_value))
    block_total = jnp.sum(weight, axis=-1)
    block_values = jnp.einsum(
        "bihk,bkhd->bihd",
        weight.astype(jnp.bfloat16),
        value_cache,
        preferred_element_type=jnp.float32,
    )
    owner = positions[None, :] == (valid - 1)[:, None]
    candidate = jnp.max(jnp.where(owner[:, :, None], cum_cache, floor_value), axis=1)
    tree_mask = (ancestors > 0.5)[:, :, None, :]
    tree_score = (
        jnp.einsum("bihd,bjhd->bihj", query, key_new, preferred_element_type=jnp.float32) * scale
        + path[..., None]
        - jnp.swapaxes(path, 1, 2)[:, None]
    )
    tree_max = jnp.max(jnp.where(tree_mask, tree_score, floor_value), axis=-1)
    tree_weight = jnp.exp(jnp.where(tree_mask, tree_score - tree_max[..., None], floor_value))
    tree_total = jnp.sum(tree_weight, axis=-1)
    tree_values = jnp.einsum(
        "bihj,bjhd->bihd",
        tree_weight.astype(jnp.bfloat16),
        value_new,
        preferred_element_type=jnp.float32,
    )
    tree_max_rows = tree_max.reshape(all_rows, heads_local)
    tree_total_rows = tree_total.reshape(all_rows, heads_local)
    tree_values_rows = tree_values.reshape(all_rows, heads_local, head_dim)
    cache_max, cache_total, cache_values, last_cum = merged(
        (block_max, block_total, block_values, candidate), "kv", combine_parts
    )
    last_rows = jnp.broadcast_to(last_cum[:, None, :], (num_seqs, proposals, heads_local)).reshape(
        all_rows, heads_local
    )
    attended = finish_rows(
        cache_max.reshape(all_rows, heads_local),
        cache_total.reshape(all_rows, heads_local),
        cache_values.reshape(all_rows, heads_local, head_dim),
        last_rows,
        tree_max_rows,
        tree_total_rows,
        tree_values_rows,
    )
    mixed_part = jnp.dot(attended, w_out, preferred_element_type=jnp.float32)
    mixed_sum = lax.psum_scatter(
        mixed_part.astype(jnp.bfloat16), "tp", scatter_dimension=1, tiled=True
    ).astype(jnp.float32)
    squares = lax.psum(jnp.sum(mixed_sum * mixed_sum, axis=1), ("kv", "tp"))
    mixed = (mixed_sum * lax.rsqrt(squares / model_width + epsilon)[:, None] * gain_post).astype(
        jnp.bfloat16
    )
    mixed = mixed.reshape(num_seqs, proposals, mixed_sum.shape[1])
    relative = positions[None, :] - valid[:, None]
    select = relative[:, :, None] == jnp.arange(proposals, dtype=jnp.int32)[None, None, :]
    written = (relative >= 0) & (relative < proposals)
    placed_keys = jnp.einsum(
        "bkj,bjhd->bkhd", select.astype(jnp.bfloat16), key_new, preferred_element_type=jnp.float32
    ).astype(jnp.bfloat16)
    placed_values = jnp.einsum(
        "bkj,bjhd->bkhd", select.astype(jnp.bfloat16), value_new, preferred_element_type=jnp.float32
    ).astype(jnp.bfloat16)
    key_out = jnp.where(written[:, :, None, None], placed_keys, key_cache)
    value_out = jnp.where(written[:, :, None, None], placed_values, value_cache)
    cum_new = last_cum[:, None, :] + path
    placed_cum = jnp.einsum(
        "bkj,bjh->bkh", select.astype(jnp.float32), cum_new, precision=lax.Precision.HIGHEST
    )
    cum_out = jnp.where(written[:, :, None], placed_cum, cum_cache)
    return (mixed, key_out, value_out, cum_out)


def solution(mesh):
    return jax.shard_map(
        per_device,
        mesh=mesh,
        in_specs=(
            P(),
            P(),
            P("kv", "tp"),
            P("kv", "tp"),
            P("kv", "tp"),
            P(),
            P(),
            P("tp", "kv"),
            P(("kv", "tp")),
            P(None, "kv", "tp", None),
            P(None, "kv", "tp", None),
            P(None, "kv", "tp"),
            P(),
            P(),
            P(),
        ),
        out_specs=(
            P(None, None, ("kv", "tp")),
            P(None, "kv", "tp", None),
            P(None, "kv", "tp", None),
            P(None, "kv", "tp"),
        ),
        check_vma=False,
    )
```

profile of v0, /device:TPU:0, one launch (start us, length us, event | category | flops | bytes accessed | tf_op | source)
XLA Modules:
  0.0 293.7 jit_solution(18166977951993972896)
XLA Ops:
  7.2 2.1 fusion.4
  9.4 2.2 fusion.6
  12.0 0.8 copy.97
  12.8 1.3 convolution_convert_fusion.1
  14.2 1.4 convolution_convert_fusion.3
  15.6 0.8 copy.87
  16.4 0.7 copy.100
  18.0 1.5 fusion.71
  20.6 75.1 %all-reduce.3.cloned.1.call-done = (bf16[16,16,4,128]{3,1,2,0:T(8,128)(2,1)}, bf16[16,16,4,128]{3,1,2,0:T(8,128)(2,1)}, bf16[16,16,4,128]{3,1,2,0:T(8,128)(2,1)}) async-done(((bf16[16,16,4,128]{3,1,2,0:T(8,128)(2,1)}, bf16[16,16,4,128]{3,1,2,0:T(8,128)(2,1)}, bf16[16,16,4,128]{3,1,2,0:T(8,128)(2,1)}), (bf16[16,16,4,128]{3,1,2,0:T(8,128)(2,1)}, bf16[16,16,4,128]{3,1,2,0:T(8,128)(2,1)}, ...) | async-done | bytes 786448 | tf_op jit(solution)/shard_map/psum | solution.py:97
  95.7 3.0 %select_reduce_fusion.1 = (f32[16,16,4]{1,2,0:T(4,128)S(1)}, f32[16,16,4,128]{3,1,2,0:T(8,128)S(1)}) fusion(pred[16,128]{1,0:T(8,128)(4,1)S(1)} %get-tuple-element.314, f32[16,4,128]{2,1,0:T(4,128)S(1)} %bitcast.132, f32[16,16,4]{1,2,0:T(4,128)S(1)} %fusion.63, bf16[16,16,4,128]{3,1,2,0:T(8,128)(2,1)} %get-tuple-element.302, ...), kind=kOutput, calls=%fused_computation.51 | convolution fusion | flops 34208768 | bytes 2926592 | tf_op jit(solution)/shard_map/bihd,bkhd->bihk/dot_general | solution.py:117
  98.7 0.8 copy-done.2
  99.5 1.5 fusion.11
  101.4 26.7 %all-gather.4 = f32[8,16,4]{1,2,0:T(4,128)S(1)} all-gather(f32[1,16,4]{1,2,0:T(4,128)S(1)} %bitcast.134), channel_id=5, replica_groups=mesh['kv'=8,'tp'=4] {'kv'}, dimensions={0}, use_global_device_ids=true | all-gather | bytes 2304 | tf_op jit(solution)/shard_map/all_gather | solution.py:11
  128.8 1.4 select_reduce_fusion
  130.5 1.0 copy.102
  131.9 32.2 %all-gather = f32[128,16,4]{1,2,0:T(4,128)S(1)} all-gather(f32[16,16,4]{1,2,0:T(4,128)S(1)} %get-tuple-element.320), channel_id=2, replica_groups=mesh['kv'=8,'tp'=4] {'kv'}, dimensions={0}, use_global_device_ids=true | all-gather | bytes 36864 | tf_op jit(solution)/shard_map/all_gather | solution.py:11
  164.1 1.5 fusion.33
  165.6 31.7 %all-gather.1 = f32[128,16,4]{1,2,0:T(4,128)S(1)} all-gather(f32[16,16,4]{1,2,0:T(4,128)S(1)} %fusion.33), channel_id=3, replica_groups=mesh['kv'=8,'tp'=4] {'kv'}, dimensions={0}, use_global_device_ids=true | all-gather | bytes 36864 | tf_op jit(solution)/shard_map/all_gather | solution.py:11
  197.2 1.0 convert_select_fusion
  198.3 3.1 %copy.110 = bf16[16,128,4,128]{3,2,1,0:T(4,128)(2,1)} copy(bf16[16,128,4,128]{3,1,2,0:T(8,128)(2,1)S(1)} %convert_select_fusion) | data formatting | bytes 4194304
  201.4 1.1 slice.11
  202.6 22.1 %while.21 = (s32[]{:T(128)}, f32[16,16,4]{1,2,0:T(4,128)S(1)}, f32[16,16,4]{1,2,0:T(4,128)S(1)}, f32[16,16,4,128]{3,2,1,0:T(4,128)S(1)}, f32[16,4]{0,1:T(4,128)S...) while((s32[]{:T(128)}, f32[16,16,4]{1,2,0:T(4,128)S(1)}, ...), condition=%wide.region_6.7_spmd, body=%wide.region_5.6_spmd.sunk | while | flops 399429 | bytes 2679715 | solution.py:16
  202.7 0.7 bitcast_maximum_fusion.4
  203.8 1.1 constant_dynamic-slice_fusion.2
  204.8 1.0 fusion.105
  205.8 0.7 bitcast_maximum_fusion.4
  206.9 1.1 constant_dynamic-slice_fusion.2
  208.0 1.0 fusion.105
  210.1 1.1 constant_dynamic-slice_fusion.2
  211.2 1.0 fusion.105
  212.1 0.7 bitcast_maximum_fusion.4
  213.2 1.1 constant_dynamic-slice_fusion.2
  214.3 1.0 fusion.105
  215.3 0.7 bitcast_maximum_fusion.4
  216.4 1.1 constant_dynamic-slice_fusion.2
  217.5 1.0 fusion.105
  219.5 1.1 constant_dynamic-slice_fusion.2
  220.6 1.0 fusion.105
  222.7 1.1 constant_dynamic-slice_fusion.2
  223.8 1.0 fusion.105
  227.0 0.8 copy.113
  227.8 2.4 convert_select_fusion.1
  230.2 3.1 %copy.109 = bf16[16,128,4,128]{3,2,1,0:T(4,128)(2,1)} copy(bf16[16,128,4,128]{3,1,2,0:T(8,128)(2,1)S(1)} %convert_select_fusion.1) | data formatting | bytes 4194304
  233.3 0.9 convolution_select_fusion
  234.2 11.8 %reduce-scatter.4.cloned.1.call-done = bf16[128,256]{1,0:T(8,128)(2,1)} async-done(((bf16[512,256]{1,0:T(8,128)(2,1)}), bf16[128,256]{1,0:T(8,128)(2,1)}) %reduce-scatter.4.cloned.1.call-update) | async-done | bytes 65552
  246.0 0.9 copy.114
  247.1 39.3 %psum.31 = f32[256]{0:T(256)S(1)} all-reduce(f32[256]{0:T(256)S(1)} %fusion.48), channel_id=1, replica_groups=mesh['kv'=8,'tp'=4] {'kv','tp'}, use_global_device_ids=true, to_apply=%region_13.14 | all-reduce | flops 256 | bytes 2048 | tf_op jit(solution)/shard_map/psum | solution.py:169
  286.4 0.7 fusion.50
  (114 shorter events, 11.4 us)
Async XLA Ops:
  7.2 4.5 %copy-start = (bf16[512,512]{1,0:T(8,128)(2,1)S(1)}, bf16[512,512]{1,0:T(8,128)(2,1)}, u32[]{:S(2)}) copy-start(bf16[512,512]{1,0:T(8,128)(2,1)} %param.20) | copy-start | bytes 1572868
  7.2 2.2 copy-start.10
  7.2 88.5 %all-reduce.3.cloned.1.call-start = ((), (), s32[]{:S(2)}) async-start(), calls=%async_computation.3 | async-start | bytes 1572864 | tf_op jit(solution)/shard_map/psum | solution.py:97
  14.1 3.2 %copy-start.17 = (s32[16,16]{1,0:T(8,128)S(1)}, s32[16,16]{1,0:T(8,128)}, u32[]{:S(2)}) copy-start(s32[16,16]{1,0:T(8,128)} %param.31) | copy-start | bytes 3076
  14.1 3.8 %copy-start.18 = (f32[16]{0:T(128)S(1)}, f32[16]{0:T(128)}, u32[]{:S(2)}) copy-start(f32[16]{0:T(128)} %param.23) | copy-start | bytes 196
  14.1 3.9 %copy-start.13 = (s32[16]{0:T(128)S(1)}, s32[16]{0:T(128)}, u32[]{:S(2)}) copy-start(s32[16]{0:T(128)} %param.29) | copy-start | bytes 196
  14.1 3.9 %copy-start.14 = (s32[16]{0:T(128)S(1)}, s32[16]{0:T(128)}, u32[]{:S(2)}) copy-start(s32[16]{0:T(128)} %param.30) | copy-start | bytes 196
  17.2 78.5 %copy-start.6 = (f32[16,128,4]{1,2,0:T(4,128)S(1)}, f32[16,128,4]{1,2,0:T(4,128)}, u32[]{:S(2)}) copy-start(f32[16,128,4]{1,2,0:T(4,128)} %param.28) | copy-start | bytes 98308
  17.2 184.2 %all-gather.7.cloned.1.call-start = ((), (), s32[]{:S(2)}) async-start(), calls=%async_computation.1 | async-start | bytes 4718592 | tf_op jit(solution)/shard_map/all_gather | solution.py:11
  19.7 79.8 %copy-start.1 = (bf16[16,128,4,128]{3,2,1,0:T(4,128)(2,1)S(1)}, bf16[16,128,4,128]{3,2,1,0:T(4,128)(2,1)}, u32[]{:S(2)}) copy-start(bf16[16,128,4,128]{3,2,1,0:T(4,128)(2,1)} %param.27) | copy-start | bytes 6291460
  20.5 108.2 %copy-start.8 = (f32[16,16,4]{1,2,0:T(4,128)}, f32[16,16,4]{1,2,0:T(4,128)S(1)}, u32[]{:S(2)}) copy-start(f32[16,16,4]{1,2,0:T(4,128)S(1)} %fusion.63) | copy-start | bytes 12292
  98.7 0.8 copy-start.2
  99.5 30.7 %copy-start.4 = (bf16[16,16,4,128]{3,1,2,0:T(8,128)(2,1)S(1)}, bf16[16,16,4,128]{3,1,2,0:T(8,128)(2,1)}, u32[]{:S(2)}) copy-start(bf16[16,16,4,128]{3,1,2,0:T(8,128)(2,1)} %get-tuple-element.303) | copy-start | bytes 786436
  101.0 144.9 %reduce-scatter.4.cloned.1.call-start = ((), (), s32[]{:S(2)}) async-start(), calls=%async_computation.2 | async-start | bytes 327680
  128.1 0.7 copy-start.5
  130.2 67.0 %copy-start.11 = (s32[16,128]{1,0:T(8,128)S(1)}, s32[16,128]{1,0:T(8,128)}, u32[]{:S(2)}) copy-start(s32[16,128]{1,0:T(8,128)} %broadcast_subtract_fusion) | copy-start | bytes 24580
  224.7 1.9 copy-start.3
  224.8 1.8 copy-start.15
  226.6 1.2 copy-start.16
  230.2 3.1 %copy-start.7 = (f32[16,128,4]{1,2,0:T(4,128)S(1)}, f32[16,128,4]{1,2,0:T(4,128)}, u32[]{:S(2)}) copy-start(f32[16,128,4]{1,2,0:T(4,128)} %param.28) | copy-start | bytes 98308
  230.2 3.1 %copy-start.9 = (f32[16,16,4]{1,2,0:T(4,128)S(1)}, f32[16,16,4]{1,2,0:T(4,128)}, u32[]{:S(2)}) copy-start(f32[16,16,4]{1,2,0:T(4,128)} %copy-done.8) | copy-start | bytes 12292
  230.2 56.1 %copy-start.12 = (f32[128]{0:T(128)S(1)}, f32[128]{0:T(128)}, u32[]{:S(2)}) copy-start(f32[128]{0:T(128)} %param.25) | copy-start | bytes 1540
Sparse Core Ops, SparseCore 0:
  17.3 78.3 all-reduce.2
  101.2 77.8 all-gather.6
  228.0 17.9 reduce-scatter.3
where the time goes:
time: 295 us; the launch traced here: 294 us
  blocking collectives  130 us (44%)
  waiting for transfers between devices  87 us (29%)
  local copies, waits for them, and re-layouts  25.7 us (9%)
  other arithmetic  19.7 us (7%)
  matrix products  16.7 us (6%)
  between operations  14.2 us (5%)
    all_gather x3, blocking collectives, merged(): gathered = jax.tree.map(lambda a: lax.all_gather(a, axis), part)  90.6 us
    psum x1, waiting for transfers between devices, per_device(): lax.psum(key_part.astype(jnp.bfloat16), 'kv').astype(jnp.float32)  75.1 us
    psum x1, blocking collectives, per_device(): squares = lax.psum(jnp.sum(mixed_sum * mixed_sum, axis=1), ('kv', 'tp'))  39.3 us
    unnamed x4, waiting for transfers between devices  11.8 us
    unnamed x42, local copies, waits for them, and re-layouts  8.8 us
    dynamic_slice x11, local copies, waits for them, and re-layouts, take(): lax.dynamic_index_in_dim(a, source, 0, False)  8.64 us
    add x7, other arithmetic, combine_parts(): first[2] * first_scale[..., None] + second[2] * second_scale[..., None]  6.66 us
  transfers between devices with their start and end apart: 3, of which 2 were waited for; matrix products, arithmetic and copies ran while one was open for 7% of the time, Pallas kernels for 0%

commit v1 on v0

--- a/solution.py
+++ b/solution.py
@@ -166,7 +166,8 @@
     mixed_sum = lax.psum_scatter(
         mixed_part.astype(jnp.bfloat16), "tp", scatter_dimension=1, tiled=True
     ).astype(jnp.float32)
-    squares = lax.psum(jnp.sum(mixed_sum * mixed_sum, axis=1), ("kv", "tp"))
+    render_target = lambda point, mesh_name: jnp.sum(lax.all_gather(point, mesh_name), axis=0)
+    squares = render_target(jnp.sum(mixed_sum * mixed_sum, axis=1), ("kv", "tp"))
     mixed = (mixed_sum * lax.rsqrt(squares / model_width + epsilon)[:, None] * gain_post).astype(
         jnp.bfloat16
     )

time: 295 us -> 296 us (level)
    all_gather x0 -> x1, blocking collectives: none -> 40.6 us  [per_device(): lax.all_gather(point, mesh_name)]
    psum x1 -> x0, blocking collectives: 39.3 us -> none  [per_device(): squares = lax.psum(jnp.sum(mixed_sum * mixed_sum, axis=1), ('kv', 'tp'))]
  transfers between devices with their start and end apart: 3 -> 3, of which waited for: 2 -> 2; matrix products, arithmetic and copies ran while one was open for 7% -> 6% of each run, Pallas kernels for 0% -> 0%
where the time goes in v1:
time: 296 us; the launch traced here: 295 us
  blocking collectives  131 us (44%)
  waiting for transfers between devices  87 us (29%)
  local copies, waits for them, and re-layouts  25.7 us (9%)
  other arithmetic  19.8 us (7%)
  matrix products  16.7 us (6%)
  between operations  14.2 us (5%)
    all_gather x3, blocking collectives, merged(): gathered = jax.tree.map(lambda a: lax.all_gather(a, axis), part)  90.6 us
    psum x1, waiting for transfers between devices, per_device(): lax.psum(key_part.astype(jnp.bfloat16), 'kv').astype(jnp.float32)  75.1 us
    all_gather x1, blocking collectives, per_device(): lax.all_gather(point, mesh_name)  40.6 us
    unnamed x4, waiting for transfers between devices  11.8 us
    unnamed x42, local copies, waits for them, and re-layouts  8.8 us
    dynamic_slice x11, local copies, waits for them, and re-layouts, take(): lax.dynamic_index_in_dim(a, source, 0, False)  8.64 us
    add x7, other arithmetic, combine_parts(): first[2] * first_scale[..., None] + second[2] * second_scale[..., None]  6.66 us
  transfers between devices with their start and end apart: 3, of which 2 were waited for; matrix products, arithmetic and copies ran while one was open for 6% of the time, Pallas kernels for 0%

profile of v1, /device:TPU:0, one launch (start us, length us, event | category | flops | bytes accessed | tf_op | source)
XLA Modules:
  0.0 295.0 jit_solution(3005657629722579693)
XLA Ops:
  7.2 2.1 fusion.4
  9.4 2.2 fusion.6
  12.0 0.8 copy.97
  12.8 1.3 convolution_convert_fusion.1
  14.2 1.4 convolution_convert_fusion.3
  15.6 0.8 copy.87
  16.4 0.7 copy.100
  18.0 1.5 fusion.71
  20.6 75.1 %all-reduce.3.cloned.1.call-done = (bf16[16,16,4,128]{3,1,2,0:T(8,128)(2,1)}, bf16[16,16,4,128]{3,1,2,0:T(8,128)(2,1)}, bf16[16,16,4,128]{3,1,2,0:T(8,128)(2,1)}) async-done(((bf16[16,16,4,128]{3,1,2,0:T(8,128)(2,1)}, bf16[16,16,4,128]{3,1,2,0:T(8,128)(2,1)}, bf16[16,16,4,128]{3,1,2,0:T(8,128)(2,1)}), (bf16[16,16,4,128]{3,1,2,0:T(8,128)(2,1)}, bf16[16,16,4,128]{3,1,2,0:T(8,128)(2,1)}, ...) | async-done | bytes 786448 | tf_op jit(solution)/shard_map/psum | solution.py:97
  95.7 3.0 %select_reduce_fusion.1 = (f32[16,16,4]{1,2,0:T(4,128)S(1)}, f32[16,16,4,128]{3,1,2,0:T(8,128)S(1)}) fusion(pred[16,128]{1,0:T(8,128)(4,1)S(1)} %get-tuple-element.314, f32[16,4,128]{2,1,0:T(4,128)S(1)} %bitcast.133, f32[16,16,4]{1,2,0:T(4,128)S(1)} %fusion.63, bf16[16,16,4,128]{3,1,2,0:T(8,128)(2,1)} %get-tuple-element.302, ...), kind=kOutput, calls=%fused_computation.51 | convolution fusion | flops 34208768 | bytes 2926592 | tf_op jit(solution)/shard_map/bihd,bkhd->bihk/dot_general | solution.py:117
  98.7 0.8 copy-done.2
  99.5 1.5 fusion.11
  101.4 26.7 %all-gather.5 = f32[8,16,4]{1,2,0:T(4,128)S(1)} all-gather(f32[1,16,4]{1,2,0:T(4,128)S(1)} %bitcast.135), channel_id=5, replica_groups=mesh['kv'=8,'tp'=4] {'kv'}, dimensions={0}, use_global_device_ids=true | all-gather | bytes 2304 | tf_op jit(solution)/shard_map/all_gather | solution.py:11
  128.8 1.4 select_reduce_fusion
  130.5 1.0 copy.102
  131.9 32.2 %all-gather = f32[128,16,4]{1,2,0:T(4,128)S(1)} all-gather(f32[16,16,4]{1,2,0:T(4,128)S(1)} %get-tuple-element.320), channel_id=2, replica_groups=mesh['kv'=8,'tp'=4] {'kv'}, dimensions={0}, use_global_device_ids=true | all-gather | bytes 36864 | tf_op jit(solution)/shard_map/all_gather | solution.py:11
  164.1 1.5 fusion.33
  165.6 31.7 %all-gather.1 = f32[128,16,4]{1,2,0:T(4,128)S(1)} all-gather(f32[16,16,4]{1,2,0:T(4,128)S(1)} %fusion.33), channel_id=3, replica_groups=mesh['kv'=8,'tp'=4] {'kv'}, dimensions={0}, use_global_device_ids=true | all-gather | bytes 36864 | tf_op jit(solution)/shard_map/all_gather | solution.py:11
  197.2 1.0 convert_select_fusion
  198.3 3.1 %copy.110 = bf16[16,128,4,128]{3,2,1,0:T(4,128)(2,1)} copy(bf16[16,128,4,128]{3,1,2,0:T(8,128)(2,1)S(1)} %convert_select_fusion) | data formatting | bytes 4194304
  201.4 1.1 slice.11
  202.6 22.1 %while.21 = (s32[]{:T(128)}, f32[16,16,4]{1,2,0:T(4,128)S(1)}, f32[16,16,4]{1,2,0:T(4,128)S(1)}, f32[16,16,4,128]{3,2,1,0:T(4,128)S(1)}, f32[16,4]{0,1:T(4,128)S...) while((s32[]{:T(128)}, f32[16,16,4]{1,2,0:T(4,128)S(1)}, ...), condition=%wide.region_6.7_spmd, body=%wide.region_5.6_spmd.sunk | while | flops 399429 | bytes 2679715 | solution.py:16
  202.7 0.7 bitcast_maximum_fusion.4
  203.8 1.1 constant_dynamic-slice_fusion.2
  204.8 1.0 fusion.105
  205.8 0.7 bitcast_maximum_fusion.4
  206.9 1.1 constant_dynamic-slice_fusion.2
  208.0 1.0 fusion.105
  210.1 1.1 constant_dynamic-slice_fusion.2
  211.2 1.0 fusion.105
  212.1 0.7 bitcast_maximum_fusion.4
  213.2 1.1 constant_dynamic-slice_fusion.2
  214.3 1.0 fusion.105
  215.3 0.7 bitcast_maximum_fusion.4
  216.4 1.1 constant_dynamic-slice_fusion.2
  217.5 1.0 fusion.105
  219.5 1.1 constant_dynamic-slice_fusion.2
  220.6 1.0 fusion.105
  222.7 1.1 constant_dynamic-slice_fusion.2
  223.8 1.0 fusion.105
  227.0 0.8 copy.113
  227.8 2.4 convert_select_fusion.1
  230.2 3.1 %copy.109 = bf16[16,128,4,128]{3,2,1,0:T(4,128)(2,1)} copy(bf16[16,128,4,128]{3,1,2,0:T(8,128)(2,1)S(1)} %convert_select_fusion.1) | data formatting | bytes 4194304
  233.3 0.9 convolution_select_fusion
  234.2 11.8 %reduce-scatter.4.cloned.1.call-done = bf16[128,256]{1,0:T(8,128)(2,1)} async-done(((bf16[512,256]{1,0:T(8,128)(2,1)}), bf16[128,256]{1,0:T(8,128)(2,1)}) %reduce-scatter.4.cloned.1.call-update) | async-done | bytes 65552
  246.0 0.9 copy.114
  247.1 40.6 %all-gather.6 = f32[32,1,256]{2,1,0:T(1,128)S(1)} all-gather(f32[1,1,256]{2,1,0:T(1,128)S(1)} %bitcast.136), channel_id=6, replica_groups=mesh['kv'=8,'tp'=4] {'kv','tp'}, dimensions={0}, use_global_device_ids=true | all-gather | bytes 33792 | tf_op jit(solution)/shard_map/all_gather | solution.py:169
  287.7 0.7 fusion.50
  (115 shorter events, 11.5 us)
Async XLA Ops:
  7.2 4.5 %copy-start = (bf16[512,512]{1,0:T(8,128)(2,1)S(1)}, bf16[512,512]{1,0:T(8,128)(2,1)}, u32[]{:S(2)}) copy-start(bf16[512,512]{1,0:T(8,128)(2,1)} %param.20) | copy-start | bytes 1572868
  7.2 2.2 copy-start.10
  7.2 88.5 %all-reduce.3.cloned.1.call-start = ((), (), s32[]{:S(2)}) async-start(), calls=%async_computation.3 | async-start | bytes 1572864 | tf_op jit(solution)/shard_map/psum | solution.py:97
  14.1 3.2 %copy-start.17 = (s32[16,16]{1,0:T(8,128)S(1)}, s32[16,16]{1,0:T(8,128)}, u32[]{:S(2)}) copy-start(s32[16,16]{1,0:T(8,128)} %param.31) | copy-start | bytes 3076
  14.1 3.8 %copy-start.18 = (f32[16]{0:T(128)S(1)}, f32[16]{0:T(128)}, u32[]{:S(2)}) copy-start(f32[16]{0:T(128)} %param.23) | copy-start | bytes 196
  14.1 3.9 %copy-start.13 = (s32[16]{0:T(128)S(1)}, s32[16]{0:T(128)}, u32[]{:S(2)}) copy-start(s32[16]{0:T(128)} %param.29) | copy-start | bytes 196
  14.1 3.9 %copy-start.14 = (s32[16]{0:T(128)S(1)}, s32[16]{0:T(128)}, u32[]{:S(2)}) copy-start(s32[16]{0:T(128)} %param.30) | copy-start | bytes 196
  17.2 78.5 %copy-start.6 = (f32[16,128,4]{1,2,0:T(4,128)S(1)}, f32[16,128,4]{1,2,0:T(4,128)}, u32[]{:S(2)}) copy-start(f32[16,128,4]{1,2,0:T(4,128)} %param.28) | copy-start | bytes 98308
  17.2 184.2 %all-gather.9.cloned.1.call-start = ((), (), s32[]{:S(2)}) async-start(), calls=%async_computation.1 | async-start | bytes 4718592 | tf_op jit(solution)/shard_map/all_gather | solution.py:11
  19.7 79.8 %copy-start.1 = (bf16[16,128,4,128]{3,2,1,0:T(4,128)(2,1)S(1)}, bf16[16,128,4,128]{3,2,1,0:T(4,128)(2,1)}, u32[]{:S(2)}) copy-start(bf16[16,128,4,128]{3,2,1,0:T(4,128)(2,1)} %param.27) | copy-start | bytes 6291460
  20.5 108.2 %copy-start.8 = (f32[16,16,4]{1,2,0:T(4,128)}, f32[16,16,4]{1,2,0:T(4,128)S(1)}, u32[]{:S(2)}) copy-start(f32[16,16,4]{1,2,0:T(4,128)S(1)} %fusion.63) | copy-start | bytes 12292
  98.7 0.8 copy-start.2
  99.5 30.7 %copy-start.4 = (bf16[16,16,4,128]{3,1,2,0:T(8,128)(2,1)S(1)}, bf16[16,16,4,128]{3,1,2,0:T(8,128)(2,1)}, u32[]{:S(2)}) copy-start(bf16[16,16,4,128]{3,1,2,0:T(8,128)(2,1)} %get-tuple-element.303) | copy-start | bytes 786436
  101.0 144.9 %reduce-scatter.4.cloned.1.call-start = ((), (), s32[]{:S(2)}) async-start(), calls=%async_computation.2 | async-start | bytes 327680
  128.1 0.7 copy-start.5
  130.2 67.0 %copy-start.11 = (s32[16,128]{1,0:T(8,128)S(1)}, s32[16,128]{1,0:T(8,128)}, u32[]{:S(2)}) copy-start(s32[16,128]{1,0:T(8,128)} %broadcast_subtract_fusion) | copy-start | bytes 24580
  224.7 1.9 copy-start.3
  224.8 1.8 copy-start.15
  226.6 1.2 copy-start.16
  230.2 3.1 %copy-start.7 = (f32[16,128,4]{1,2,0:T(4,128)S(1)}, f32[16,128,4]{1,2,0:T(4,128)}, u32[]{:S(2)}) copy-start(f32[16,128,4]{1,2,0:T(4,128)} %param.28) | copy-start | bytes 98308
  230.2 3.1 %copy-start.9 = (f32[16,16,4]{1,2,0:T(4,128)S(1)}, f32[16,16,4]{1,2,0:T(4,128)}, u32[]{:S(2)}) copy-start(f32[16,16,4]{1,2,0:T(4,128)} %copy-done.8) | copy-start | bytes 12292
  230.2 57.5 %copy-start.12 = (f32[128]{0:T(128)S(1)}, f32[128]{0:T(128)}, u32[]{:S(2)}) copy-start(f32[128]{0:T(128)} %param.25) | copy-start | bytes 1540
Sparse Core Ops, SparseCore 0:
  17.3 78.3 all-reduce.2
  101.2 77.8 all-gather.8
  228.0 17.9 reduce-scatter.3
